TPU v7x, 32 devices: a whole 2x2x4 slice. The times are simulated.
32 devices in a mesh: grp: 2 (over x), fs: 4 (over y, core), tp: 4 (over z).
Axes of the slice: x: 2, y: 2, z: 4, core: 2. Of those that a mesh axis runs over, the one named last changes fastest.
Arguments:
- stream: bfloat16 [4096, 2048], P(('grp', 'fs', 'tp')), parts along dimension 0, may hold values from -4 to 4
- gain_first: bfloat16 [2048], replicated, may hold values from 0.099609375 to 1.8984375
- gate_first: bfloat16 [2048, 4096], P('fs', 'tp'), may hold values from -0.125 to 0.125
- up_first: bfloat16 [2048, 4096], P('fs', 'tp'), may hold values from -0.125 to 0.125
- down_first: bfloat16 [4096, 2048], P('tp', 'fs'), may hold values from -0.09375 to 0.09375
- gain_second: bfloat16 [2048], replicated, may hold values from 0.099609375 to 1.8984375
- gate_second: bfloat16 [2048, 4096], P('fs', 'tp'), may hold values from -0.125 to 0.125
- up_second: bfloat16 [2048, 4096], P('fs', 'tp'), may hold values from -0.125 to 0.125
- down_second: bfloat16 [4096, 2048], P('tp', 'fs'), may hold values from -0.09375 to 0.09375
Outputs:
- result: bfloat16 [4096, 2048], P(('grp', 'fs', 'tp')), parts along dimension 0
There are 2 independent parts, one for each index of `grp`. A program takes and returns all parts, laid end to end along the dimension named above; an argument that names none is the same for every part. Nothing has to cross between parts.
All inputs are finite; a program needn't handle non-finite values.
Results may differ from a plain program's by a relative error of at most 0.018.
Values may be sent and summed in bfloat16 or wider, within the bound.
A program may use at most 64 MiB of HBM per device.

v0:
```python
import functools

import jax
import jax.numpy as jnp
from jax import lax
from jax.experimental import pallas as pl
from jax.experimental.pallas import tpu as pltpu
from jax.sharding import PartitionSpec as P

MESH = pl.DeviceIdType.MESH
CORES = 2
PIECES = 2
VMEM_LIMIT = 60 * 1024 * 1024


def kernel(
    sizes,
    stream, gain_a, gain_b, gate_a, up_a, down_a, gate_b, up_b, down_b,
    out,
    gu, dn, xg, hid, part, rbuf, acc, mid,
    y_s, y_r, x_s, x_r, c_s, c_r, f_s, f_r, l_s, ag_s, ag_r, rs_s, rs_r,
):
    G, m, n, T, D, F, J = sizes
    Y = m // CORES
    C = D // J
    weights = (gate_a, up_a, down_a, gate_b, up_b, down_b)
    gains = (gain_a, gain_b)
    g = lax.axis_index("grp")
    fs = lax.axis_index("fs")
    me = lax.axis_index("tp")
    y = fs // CORES
    c = lax.rem(fs, CORES)
    mate = y * CORES + (CORES - 1 - c)
    right = lax.rem(me + 1, n)
    left = lax.rem(me + n - 1, n)

    def row_of(k):
        return lax.rem(y + k + Y, Y) * CORES + c

    def grp_of(i):
        return lax.rem(g + i + G, G)

    barrier = pltpu.get_barrier_semaphore()
    for k in range(1, Y):
        pl.semaphore_signal(barrier, inc=1, device_id={"fs": row_of(k)}, device_id_type=MESH)
    for i in range(1, G):
        pl.semaphore_signal(barrier, inc=1, device_id={"grp": grp_of(i)}, device_id_type=MESH)
    pl.semaphore_signal(barrier, inc=1, device_id={"fs": mate}, device_id_type=MESH)

    @pl.when(me < n - 1)
    def _():
        pl.semaphore_signal(barrier, inc=1, device_id={"tp": right}, device_id_type=MESH)

    @pl.when(me > 0)
    def _():
        pl.semaphore_signal(barrier, inc=1, device_id={"tp": left}, device_id_type=MESH)

    @pl.when(jnp.logical_and(me > 0, me < n - 1))
    def _():
        pl.semaphore_wait(barrier, Y - 1 + G - 1 + 1 + 2)

    @pl.when(jnp.logical_not(jnp.logical_and(me > 0, me < n - 1)))
    def _():
        pl.semaphore_wait(barrier, Y - 1 + G - 1 + 1 + 1)

    def rows_of(a):
        return weights[a].shape[0]

    def piece_rows(u, h):
        rows = rows_of(u // PIECES) // G
        sub = rows // PIECES
        return pl.multiple_of(h * rows + (u % PIECES) * sub, sub), sub

    def own(u, h):
        off, sub = piece_rows(u, h)
        return weights[u // PIECES].at[pl.ds(off, sub), :]

    def place(a, j, off, count):
        b, t = a // 3, a % 3
        if t < 2:
            return gu.at[b, t, pl.ds(pl.multiple_of(j * rows_of(a) + off, count), count), :]
        cols = D // m
        return dn.at[b, pl.ds(off, count), pl.ds(pl.multiple_of(j * cols, cols), cols)]

    def slot(u, j, h):
        off, sub = piece_rows(u, h)
        return place(u // PIECES, j, off, sub)

    def whole(a, j):
        return place(a, j, 0, rows_of(a))

    def remote(src, dst, ss, rs, dev):
        return pltpu.make_async_remote_copy(
            src_ref=src, dst_ref=dst, send_sem=ss, recv_sem=rs, device_id=dev, device_id_type=MESH
        )

    def local_copy(a):
        return pltpu.make_async_copy(weights[a], whole(a, fs), l_s.at[a])

    def y_copy(a, k):
        return remote(own(a, g), slot(a, fs, g), y_s.at[a, k - 1], y_r.at[a, k - 1], {"fs": row_of(k)})

    def y_arrived(a, k):
        remote(own(a, g), slot(a, row_of(-k), g), y_s.at[a, k - 1], y_r.at[a, k - 1], {"fs": row_of(k)}).wait_recv()

    def c_copy(a):
        return remote(weights[a], whole(a, fs), c_s.at[a], c_r.at[a], {"fs": mate})

    def c_arrived(a):
        remote(weights[a], whole(a, mate), c_s.at[a], c_r.at[a], {"fs": mate}).wait_recv()

    def x_copy(a, k, i):
        where = slot(a, row_of(-k), g)
        return remote(where, where, x_s.at[a, k - 1, i - 1], x_r.at[a, k - 1, i - 1], {"grp": grp_of(i)})

    def x_arrived(a, k, i):
        where = slot(a, row_of(-k), grp_of(-i))
        remote(where, where, x_s.at[a, k - 1, i - 1], x_r.at[a, k - 1, i - 1], {"grp": grp_of(i)}).wait_recv()

    def f_copy(a, k, i):
        where = slot(a, row_of(-k), grp_of(-i))
        return remote(where, where, f_s.at[a, k - 1, i], f_r.at[a, k - 1, i], {"fs": mate})

    def f_arrived(a, k, i):
        row = lax.rem(y - k + Y, Y) * CORES + (CORES - 1 - c)
        where = slot(a, row, grp_of(-i))
        remote(where, where, f_s.at[a, k - 1, i], f_r.at[a, k - 1, i], {"fs": mate}).wait_recv()

    def y_event(a):
        for k in range(1, Y):
            y_arrived(a, k)
            for i in range(1, G):
                x_copy(a, k, i).start()
            f_copy(a, k, 0).start()

    def x_event(a):
        for k in range(1, Y):
            for i in range(1, G):
                x_arrived(a, k, i)
                f_copy(a, k, i).start()

    def complete(a):
        local_copy(a).wait()
        c_arrived(a)
        for u in range(a * PIECES, (a + 1) * PIECES):
            for k in range(1, Y):
                for i in range(G):
                    f_arrived(u, k, i)

    def block(b, blk):
        return xg.at[b, pl.ds(pl.multiple_of(blk * T, T), T), :]

    def ag(b, way, blk):
        where = block(b, blk)
        return remote(where, where, ag_s.at[b, way, blk], ag_r.at[b, blk], {"tp": right if way == 0 else left})

    def ag_step(b, s, way, then=None):
        blk = me - s if way == 0 else me + s

        @pl.when(blk >= 0 if way == 0 else blk < n)
        def _():
            ag(b, way, blk).wait_recv()

            @pl.when(me < n - 1 if way == 0 else me > 0)
            def _():
                ag(b, way, blk).start()

            if then is not None:
                then(blk)

    def send_own(b):
        @pl.when(me < n - 1)
        def _():
            ag(b, 0, me).start()

        @pl.when(me > 0)
        def _():
            ag(b, 1, me).start()

    def normalize(b, source):
        step = min(32, T)

        @pl.loop(0, T // step)
        def _(r):
            rows = pl.ds(pl.multiple_of(r * step, step), step)
            v = source[rows, :].astype(jnp.float32)
            scale = lax.rsqrt(jnp.mean(v * v, axis=-1, keepdims=True) + 1e-06)
            dst = pl.ds(pl.multiple_of(me * T + r * step, step), step)
            xg[b, dst, :] = (v * scale * gains[b][...].astype(jnp.float32)).astype(jnp.bfloat16)

    tile = min(256, F)

    def hidden_of(b, blk):
        @pl.loop(0, F // tile)
        def _(q):
            cols = pl.ds(pl.multiple_of(q * tile, tile), tile)
            rows = pl.ds(pl.multiple_of(blk * T, T), T)
            x = xg[b, rows, :]
            gate = jnp.dot(x, gu[b, 0, :, cols], preferred_element_type=jnp.float32)
            up = jnp.dot(x, gu[b, 1, :, cols], preferred_element_type=jnp.float32)
            hid[rows, cols] = (gate / (1.0 + jnp.exp(-gate)) * up).astype(jnp.bfloat16)

    def rs(b, way, d, j):
        return remote(
            part.at[b, d, j], rbuf.at[b, way, d, j], rs_s.at[b, d, j], rs_r.at[b, way, d, j],
            {"tp": right if way == 0 else left},
        )

    def chunk_of(b, blk, j):
        cols = pl.ds(pl.multiple_of(j * C, C), C)
        rows = pl.ds(pl.multiple_of(blk * T, T), T)
        part[b, blk, j] = jnp.dot(
            hid[rows, :], dn[b, :, cols], preferred_element_type=jnp.float32
        ).astype(jnp.bfloat16)

        @pl.when(jnp.logical_and(me == 0, blk > me))
        def _():
            rs(b, 0, blk, j).start()

        @pl.when(jnp.logical_and(me == n - 1, blk < me))
        def _():
            rs(b, 1, blk, j).start()

    def partial_of(b, blk):
        @pl.loop(0, J)
        def _(j):
            chunk_of(b, blk, j)

    def relay(b, j, to_right, to_left):
        for way, d, ok in (
            (0, to_right, jnp.logical_and(me > 0, to_right > me)),
            (1, to_left, jnp.logical_and(me < n - 1, to_left < me)),
        ):
            @pl.when(ok)
            def _():
                rs(b, way, d, j).wait_recv()
                part[b, d, j] = (
                    part[b, d, j].astype(jnp.float32) + rbuf[b, way, d, j].astype(jnp.float32)
                ).astype(jnp.bfloat16)
                rs(b, way, d, j).start()

    def finish(b, source, target):
        @pl.loop(0, J)
        def _(j):
            cols = pl.ds(pl.multiple_of(j * C, C), C)
            acc[...] = part[b, me, j].astype(jnp.float32)

            @pl.when(me > 0)
            def _():
                rs(b, 0, me, j).wait_recv()
                acc[...] += rbuf[b, 0, me, j].astype(jnp.float32)

            @pl.when(me < n - 1)
            def _():
                rs(b, 1, me, j).wait_recv()
                acc[...] += rbuf[b, 1, me, j].astype(jnp.float32)

            target[:, cols] = (source[:, cols].astype(jnp.float32) + 0.5 * acc[...]).astype(jnp.bfloat16)

    for u in range(6 * PIECES):
        for k in range(1, Y):
            y_copy(u, k).start()
    normalize(0, stream)
    send_own(0)
    for a in range(6):
        local_copy(a).start()
        c_copy(a).start()

    events = [("y", 0)]
    for u in range(1, 6 * PIECES):
        events += [("y", u), ("x", u - 1)]
    events += [("x", 6 * PIECES - 1)]

    def run(last=None, count=0):
        stop = events.index(last) + 1 if last in events else (0 if last else min(count, len(events)))
        for kind, u in events[:stop]:
            (y_event if kind == "y" else x_event)(u)
        del events[:stop]

    def hidden_pair(b, first, last):
        @pl.loop(first, last)
        def _(s):
            for blk, ok in ((me - s, me - s >= 0), (me + s, me + s < n)):
                @pl.when(ok)
                def _():
                    hidden_of(b, blk)

    run(("x", 0))
    for s in range(1, n - 1):
        ag_step(0, s, 0)
        ag_step(0, s, 1)
        if s == 1:
            run(("x", 2 * PIECES - 2))
    run(("x", 2 * PIECES - 1))
    complete(0)
    complete(1)
    hidden_of(0, me)
    hidden_pair(0, 1, min(2, n - 1))
    run(("x", 3 * PIECES - 2))
    ag_step(0, n - 1, 0)
    ag_step(0, n - 1, 1)
    hidden_pair(0, min(2, n - 1), n)
    run(("x", 3 * PIECES - 1))
    complete(2)
    upper = lax.div(me, (n + 1) // 2)
    for j in range(J):
        @pl.loop(0, n)
        def _(t):
            chunk_of(0, t + (1 - upper) * (n - 1 - 2 * t), j)

        @pl.loop(1, n)
        def _(q):
            relay(0, j, n - q, q - 1)

        if j < J - 1:
            run(None, 4)
    run(None, len(events))
    finish(0, stream, mid)
    normalize(1, mid)
    send_own(1)
    complete(3)
    complete(4)
    complete(5)

    def both(blk):
        hidden_of(1, blk)
        partial_of(1, blk)

    both(me)
    for s in range(1, n):
        ag_step(1, s, 0, both)
        ag_step(1, s, 1, both)
    for q in range(1, n):
        @pl.loop(0, J)
        def _(j):
            relay(1, j, q, n - 1 - q)

    finish(1, mid, out)

    for a in range(6):
        c_copy(a).wait_send()
    for u in range(6 * PIECES):
        for k in range(1, Y):
            y_copy(u, k).wait_send()
            f_copy(u, k, 0).wait_send()
            for i in range(1, G):
                x_copy(u, k, i).wait_send()
                f_copy(u, k, i).wait_send()

    for b in range(2):
        @pl.loop(0, n)
        def _(d):
            @pl.when(jnp.logical_and(d <= me, me < n - 1))
            def _():
                ag(b, 0, d).wait_send()

            @pl.when(jnp.logical_and(d >= me, me > 0))
            def _():
                ag(b, 1, d).wait_send()

            @pl.loop(0, J)
            def _(j):
                @pl.when(d > me)
                def _():
                    rs(b, 0, d, j).wait_send()

                @pl.when(d < me)
                def _():
                    rs(b, 1, d, j).wait_send()


def local(sizes_of_mesh, stream, gain_a, gate_a, up_a, down_a, gain_b, gate_b, up_b, down_b):
    G, m, n = sizes_of_mesh
    T, D = stream.shape
    F = gate_a.shape[1]
    J = 4 if D % 512 == 0 else 1
    Y = m // CORES
    U = 6 * PIECES
    bf16 = jnp.bfloat16
    vmem = pl.BlockSpec(memory_space=pltpu.VMEM)
    anywhere = pl.BlockSpec(memory_space=pl.ANY)
    dma = pltpu.SemaphoreType.DMA
    return pl.pallas_call(
        functools.partial(kernel, (G, m, n, T, D, F, J)),
        out_shape=jax.ShapeDtypeStruct((T, D), bf16),
        in_specs=[vmem] * 3 + [anywhere] * 6,
        out_specs=vmem,
        scratch_shapes=[
            pltpu.VMEM((2, 2, D, F), bf16),
            pltpu.VMEM((2, F, D), bf16),
            pltpu.VMEM((2, n * T, D), bf16),
            pltpu.VMEM((n * T, F), bf16),
            pltpu.VMEM((2, n, J, T, D // J), bf16),
            pltpu.VMEM((2, 2, n, J, T, D // J), bf16),
            pltpu.VMEM((T, D // J), jnp.float32),
            pltpu.VMEM((T, D), bf16),
            dma((U, Y - 1)), dma((U, Y - 1)),
            dma((U, Y - 1, G - 1)), dma((U, Y - 1, G - 1)),
            dma((6,)), dma((6,)),
            dma((U, Y - 1, G)), dma((U, Y - 1, G)),
            dma((6,)),
            dma((2, 2, n)), dma((2, n)),
            dma((2, n, J)), dma((2, 2, n, J)),
        ],
        compiler_params=pltpu.CompilerParams(
            collective_id=0, has_side_effects=True, vmem_limit_bytes=VMEM_LIMIT
        ),
    )(
        stream, gain_a.reshape(1, D), gain_b.reshape(1, D),
        gate_a, up_a, down_a, gate_b, up_b, down_b,
    )


def solution(mesh):
    shape = mesh.shape
    in_specs = (
        P(("grp", "fs", "tp"), None),
        P(),
        P("fs", "tp"),
        P("fs", "tp"),
        P("tp", "fs"),
        P(),
        P("fs", "tp"),
        P("fs", "tp"),
        P("tp", "fs"),
    )
    out_specs = P(("grp", "fs", "tp"), None)
    body = functools.partial(local, (shape["grp"], shape["fs"], shape["tp"]))
    return jax.shard_map(body, mesh=mesh, in_specs=in_specs, out_specs=out_specs, check_vma=False)
```

profile of v0, /device:TPU:0, one launch (start us, length us, event | category | flops | bytes accessed | tf_op | source)
XLA Modules:
  0.0 206.0 jit_solution(10289272321181192156)
XLA Ops:
  0.0 0.0 copy-start
  0.0 1.3 reshape.6.gain_a
  1.3 0.0 copy-done
  1.3 0.6 reshape.7.gain_b
  1.9 202.2 %shard_map.91 = bf16[128,2048]{1,0:T(8,128)(2,1)} custom-call(bf16[128,2048]{1,0:T(8,128)(2,1)} %stream.1, bf16[1,2048]{1,0:T(2,128)(2,1)} %reshape.6.gain_a, bf16[1,2048]{1,0:T(2,128)(2,1)} %reshape.7.gain_b, bf16[512,1024]{1,0:T(8,128)(2,1)} %gate_a.1, bf16[512,1024]{1,0:T(8,128)(2,1)} %up_a.1, bf16[1024,512]{1,0:T(8,128)(2,1)} %down_a.1, ...), custom_call_target="tpu_custom_call" | custom-call | tf_op jit(solution)/shard_map/pallas_call | solution.py:383
  204.1 1.9 copy.11
Async XLA Ops:
  0.0 1.3 copy-start
where the time goes:
time: 206 us
  Pallas kernels  202 us (98%)
  local copies, waits for them, and re-layouts  3.79 us (2%)
    pallas_call x1, Pallas kernels, local(): pl.pallas_call(functools.partial(kernel, (G, m, n, T, D, F, J)), out_shap...  202 us

commit v1 on v0

v1 whole, which is shorter than its diff:
```python
import functools

import jax
import jax.numpy as jnp
from jax import lax
from jax.experimental import pallas as pl
from jax.experimental.pallas import tpu as pltpu
from jax.sharding import PartitionSpec as P

MESH = pl.DeviceIdType.MESH
CORES = 2
PIECES = 4
BATCHES = 4
SLOT = 1.2
LAG = 3.2
HOP = 3.0
VMEM_LIMIT = 60 * 1024 * 1024


def kernel(
    sizes,
    stream, gain_a, gain_b, gate_a, up_a, down_a, gate_b, up_b, down_b,
    out,
    gu, dn, xg, hid, part, rbuf, acc, mid,
    y_s, y_r, x_s, x_r, c_s, c_r, f_s, f_r, l_s, ag_s, ag_r, rs_s, rs_r,
):
    G, m, n, T, D, F, J, K = sizes
    Y = m // CORES
    C = D // J
    R = T // K
    U = 6 * PIECES
    weights = (gate_a, up_a, down_a, gate_b, up_b, down_b)
    gains = (gain_a, gain_b)
    g = lax.axis_index("grp")
    fs = lax.axis_index("fs")
    me = lax.axis_index("tp")
    y = fs // CORES
    c = lax.rem(fs, CORES)
    mate = y * CORES + (CORES - 1 - c)
    right = lax.rem(me + 1, n)
    left = lax.rem(me + n - 1, n)

    def row_of(k):
        return lax.rem(y + k + Y, Y) * CORES + c

    def grp_of(i):
        return lax.rem(g + i + G, G)

    barrier = pltpu.get_barrier_semaphore()
    for k in range(1, Y):
        pl.semaphore_signal(barrier, inc=1, device_id={"fs": row_of(k)}, device_id_type=MESH)
    for i in range(1, G):
        pl.semaphore_signal(barrier, inc=1, device_id={"grp": grp_of(i)}, device_id_type=MESH)
    pl.semaphore_signal(barrier, inc=1, device_id={"fs": mate}, device_id_type=MESH)

    @pl.when(me < n - 1)
    def _():
        pl.semaphore_signal(barrier, inc=1, device_id={"tp": right}, device_id_type=MESH)

    @pl.when(me > 0)
    def _():
        pl.semaphore_signal(barrier, inc=1, device_id={"tp": left}, device_id_type=MESH)

    @pl.when(jnp.logical_and(me > 0, me < n - 1))
    def _():
        pl.semaphore_wait(barrier, Y - 1 + G - 1 + 1 + 2)

    @pl.when(jnp.logical_not(jnp.logical_and(me > 0, me < n - 1)))
    def _():
        pl.semaphore_wait(barrier, Y - 1 + G - 1 + 1 + 1)

    def rows_of(a):
        return weights[a].shape[0]

    def piece_rows(u, h):
        rows = rows_of(u // PIECES) // G
        sub = rows // PIECES
        return pl.multiple_of(h * rows + (u % PIECES) * sub, sub), sub

    def own(u, h):
        off, sub = piece_rows(u, h)
        return weights[u // PIECES].at[pl.ds(off, sub), :]

    def place(a, j, off, count):
        b, t = a // 3, a % 3
        if t < 2:
            return gu.at[b, t, pl.ds(pl.multiple_of(j * rows_of(a) + off, count), count), :]
        cols = D // m
        return dn.at[b, pl.ds(off, count), pl.ds(pl.multiple_of(j * cols, cols), cols)]

    def slot(u, j, h):
        off, sub = piece_rows(u, h)
        return place(u // PIECES, j, off, sub)

    def whole(a, j):
        return place(a, j, 0, rows_of(a))

    def remote(src, dst, ss, rs, dev):
        return pltpu.make_async_remote_copy(
            src_ref=src, dst_ref=dst, send_sem=ss, recv_sem=rs, device_id=dev, device_id_type=MESH
        )

    def local_copy(a):
        return pltpu.make_async_copy(weights[a], whole(a, fs), l_s.at[a])

    def y_copy(a, k):
        return remote(own(a, g), slot(a, fs, g), y_s.at[a, k - 1], y_r.at[a, k - 1], {"fs": row_of(k)})

    def y_arrived(a, k):
        remote(own(a, g), slot(a, row_of(-k), g), y_s.at[a, k - 1], y_r.at[a, k - 1], {"fs": row_of(k)}).wait_recv()

    def c_copy(a):
        return remote(weights[a], whole(a, fs), c_s.at[a], c_r.at[a], {"fs": mate})

    def c_arrived(a):
        remote(weights[a], whole(a, mate), c_s.at[a], c_r.at[a], {"fs": mate}).wait_recv()

    def x_copy(a, k, i):
        where = slot(a, row_of(-k), g)
        return remote(where, where, x_s.at[a, k - 1, i - 1], x_r.at[a, k - 1, i - 1], {"grp": grp_of(i)})

    def x_arrived(a, k, i):
        where = slot(a, row_of(-k), grp_of(-i))
        remote(where, where, x_s.at[a, k - 1, i - 1], x_r.at[a, k - 1, i - 1], {"grp": grp_of(i)}).wait_recv()

    def f_copy(a, k, i):
        where = slot(a, row_of(-k), grp_of(-i))
        return remote(where, where, f_s.at[a, k - 1, i], f_r.at[a, k - 1, i], {"fs": mate})

    def f_arrived(a, k, i):
        row = lax.rem(y - k + Y, Y) * CORES + (CORES - 1 - c)
        where = slot(a, row, grp_of(-i))
        remote(where, where, f_s.at[a, k - 1, i], f_r.at[a, k - 1, i], {"fs": mate}).wait_recv()

    def y_event(a):
        for k in range(1, Y):
            y_arrived(a, k)
            for i in range(1, G):
                x_copy(a, k, i).start()
            f_copy(a, k, 0).start()

    def x_event(a):
        for k in range(1, Y):
            for i in range(1, G):
                x_arrived(a, k, i)
                f_copy(a, k, i).start()

    def nearby(a):
        local_copy(a).wait()
        c_arrived(a)

    def complete(a):
        for u in range(a * PIECES, (a + 1) * PIECES):
            for k in range(1, Y):
                for i in range(G):
                    f_arrived(u, k, i)

    def rows_at(blk):
        return pl.ds(pl.multiple_of(blk * R, R), R)

    def cols_at(j):
        return pl.ds(pl.multiple_of(lax.rem(y + j, J) * C, C), C)

    def ag(b, way, k, blk):
        where = xg.at[b, k, rows_at(blk), :]
        return remote(where, where, ag_s.at[b, way, k, blk], ag_r.at[b, k, blk], {"tp": right if way == 0 else left})

    def ag_step(b, k, s):
        for way in range(2):
            blk = me - s if way == 0 else me + s

            @pl.when(blk >= 0 if way == 0 else blk < n)
            def _():
                ag(b, way, k, blk).wait_recv()

                @pl.when(me < n - 1 if way == 0 else me > 0)
                def _():
                    ag(b, way, k, blk).start()

    def normalize(b, k, source):
        rows = pl.ds(k * R, R)
        v = source[rows, :].astype(jnp.float32)
        scale = lax.rsqrt(jnp.mean(v * v, axis=-1, keepdims=True) + 1e-06)
        xg[b, k, rows_at(me), :] = (v * scale * gains[b][...].astype(jnp.float32)).astype(jnp.bfloat16)

        @pl.when(me < n - 1)
        def _():
            ag(b, 0, k, me).start()

        @pl.when(me > 0)
        def _():
            ag(b, 1, k, me).start()

    def hidden_of(b, k):
        tile = min(512, F)

        @pl.loop(0, F // tile)
        def _(q):
            cols = pl.ds(pl.multiple_of(q * tile, tile), tile)
            x = xg[b, k]
            gate = jnp.dot(x, gu[b, 0, :, cols], preferred_element_type=jnp.float32)
            up = jnp.dot(x, gu[b, 1, :, cols], preferred_element_type=jnp.float32)
            hid[k, :, cols] = (gate / (1.0 + jnp.exp(-gate)) * up).astype(jnp.bfloat16)

    def rs(b, way, k, j, d):
        return remote(
            part.at[b, k, j, rows_at(d), :], rbuf.at[b, way, k, j, rows_at(d), :],
            rs_s.at[b, k, j, d], rs_r.at[b, way, k, j, d], {"tp": right if way == 0 else left},
        )

    def partial_of(b, k, j):
        tile = min(512, C)

        @pl.loop(0, C // tile)
        def _(q):
            cols = pl.ds(pl.multiple_of(lax.rem(y + j, J) * C + q * tile, tile), tile)
            dst = pl.ds(pl.multiple_of(q * tile, tile), tile)
            part[b, k, j, :, dst] = jnp.dot(
                hid[k], dn[b, :, cols], preferred_element_type=jnp.float32
            ).astype(jnp.bfloat16)

        @pl.when(me == 0)
        def _():
            for d in range(n - 1, 0, -1):
                rs(b, 0, k, j, d).start()

        @pl.when(me == n - 1)
        def _():
            for d in range(n - 1):
                rs(b, 1, k, j, d).start()

    def relay_one(b, way, k, j, d):
        rs(b, way, k, j, d).wait_recv()
        part[b, k, j, rows_at(d), :] = (
            part[b, k, j, rows_at(d), :].astype(jnp.float32)
            + rbuf[b, way, k, j, rows_at(d), :].astype(jnp.float32)
        ).astype(jnp.bfloat16)
        rs(b, way, k, j, d).start()

    def relay(b, k, j, q):
        @pl.when(me == q)
        def _():
            @pl.loop(0, n - 1 - q)
            def _(i):
                relay_one(b, 0, k, j, n - 1 - i)

        @pl.when(n - 1 - me == q)
        def _():
            @pl.loop(0, n - 1 - q)
            def _(i):
                relay_one(b, 1, k, j, i)

    def finish(b, k, j, source, target):
        rows = pl.ds(k * R, R)
        acc[...] = part[b, k, j, rows_at(me), :].astype(jnp.float32)

        @pl.when(me > 0)
        def _():
            rs(b, 0, k, j, me).wait_recv()
            acc[...] += rbuf[b, 0, k, j, rows_at(me), :].astype(jnp.float32)

        @pl.when(me < n - 1)
        def _():
            rs(b, 1, k, j, me).wait_recv()
            acc[...] += rbuf[b, 1, k, j, rows_at(me), :].astype(jnp.float32)

        target[rows, cols_at(j)] = (
            source[rows, cols_at(j)].astype(jnp.float32) + 0.5 * acc[...]
        ).astype(jnp.bfloat16)

    for u in range(U):
        for k in range(1, Y):
            y_copy(u, k).start()
    for k in range(K):
        normalize(0, k, stream)
    for a in range(6):
        local_copy(a).start()
        c_copy(a).start()

    for kind, args in plan(n, J, K):
        with jax.named_scope(kind + "_" + "_".join(map(str, args))):
            if kind == "y":
                y_event(*args)
            elif kind == "x":
                x_event(*args)
            elif kind == "c":
                complete(*args)
            elif kind == "o":
                nearby(*args)
            elif kind == "a":
                ag_step(*args)
            elif kind == "h":
                hidden_of(*args)
            elif kind == "p":
                partial_of(*args)
            elif kind == "r":
                relay(*args)
            elif kind == "f":
                finish(*args, *((stream, mid) if args[0] == 0 else (mid, out)))
            elif kind == "n":
                normalize(*args, mid)

    for a in range(6):
        c_copy(a).wait_send()
    for u in range(U):
        for k in range(1, Y):
            y_copy(u, k).wait_send()
            f_copy(u, k, 0).wait_send()
            for i in range(1, G):
                x_copy(u, k, i).wait_send()
                f_copy(u, k, i).wait_send()

    @pl.loop(0, 2)
    def _(b):
        @pl.loop(0, K)
        def _(k):
            @pl.loop(0, n)
            def _(d):
                @pl.when(jnp.logical_and(d <= me, me < n - 1))
                def _():
                    ag(b, 0, k, d).wait_send()

                @pl.when(jnp.logical_and(d >= me, me > 0))
                def _():
                    ag(b, 1, k, d).wait_send()

                @pl.loop(0, J)
                def _(j):
                    @pl.when(d > me)
                    def _():
                        rs(b, 0, k, j, d).wait_send()

                    @pl.when(d < me)
                    def _():
                        rs(b, 1, k, j, d).wait_send()


def plan(n, J, K):
    items = []

    def at(time, kind, *args):
        items.append((time, len(items), kind, args))

    U = 6 * PIECES
    whole = J * K
    tau = whole / PIECES
    for u in range(U):
        at(tau * (u + 1) + 0.3, "y", u)
        at(tau * (u + 2) + 0.7, "x", u)
    for s in range(1, n):
        for k in range(K):
            at(whole * (s - 1) + J * (k + 1) + 0.5, "a", 0, k, s)
    ready = [tau * ((a + 1) * PIECES + 1) + 0.8 for a in range(6)]
    for a in range(6):
        at(ready[a], "c", a)
        at(0.2 + whole * a / 8, "o", a)
    slot = (n - 1) * SLOT
    order = []
    for k in range(0, K, 2):
        pair = range(k, min(k + 2, K))
        order += [(q, j) for j in range(J) for q in pair] if k == 0 else [(q, j) for q in pair for j in range(J)]
    start = ready[1] + 0.1
    arrived = [whole * (n - 2) + J * (k + 1) + 0.6 for k in range(K)]
    for b in range(2):
        begun = set()
        done = [0] * K
        now = start
        for k, j in order:
            now = max(now, arrived[k], ready[3 * b + 2] if j > 0 else 0)
            if k not in begun:
                begun.add(k)
                at(now + 0.01, "h", b, k)
            at(now + 0.02, "p", b, k, j)
            for q in range(1, n - 1):
                at(now + LAG * q, "r", b, k, j, q)
            at(now + LAG * (n - 1), "f", b, k, j)
            done[k] = max(done[k], now + LAG * (n - 1))
            now += slot
        if b == 0:
            for k in range(K):
                at(done[k] + 0.03, "n", 1, k)
                for s in range(1, n):
                    at(done[k] + 0.04 + HOP * s, "a", 1, k, s)
                arrived[k] = done[k] + 0.05 + HOP * (n - 1)
            start = max(now, ready[4] + 0.1)
    items.sort(key=lambda item: item[:2])
    return [item[2:] for item in items]


def local(sizes_of_mesh, stream, gain_a, gate_a, up_a, down_a, gain_b, gate_b, up_b, down_b):
    G, m, n = sizes_of_mesh
    T, D = stream.shape
    F = gate_a.shape[1]
    Y = m // CORES
    J = Y if Y <= 2 else 1
    K = BATCHES
    U = 6 * PIECES
    bf16 = jnp.bfloat16
    vmem = pl.BlockSpec(memory_space=pltpu.VMEM)
    anywhere = pl.BlockSpec(memory_space=pl.ANY)
    dma = pltpu.SemaphoreType.DMA
    return pl.pallas_call(
        functools.partial(kernel, (G, m, n, T, D, F, J, K)),
        out_shape=jax.ShapeDtypeStruct((T, D), bf16),
        in_specs=[vmem] * 3 + [anywhere] * 6,
        out_specs=vmem,
        scratch_shapes=[
            pltpu.VMEM((2, 2, D, F), bf16),
            pltpu.VMEM((2, F, D), bf16),
            pltpu.VMEM((2, K, n * T // K, D), bf16),
            pltpu.VMEM((K, n * T // K, F), bf16),
            pltpu.VMEM((2, K, J, n * T // K, D // J), bf16),
            pltpu.VMEM((2, 2, K, J, n * T // K, D // J), bf16),
            pltpu.VMEM((T // K, D // J), jnp.float32),
            pltpu.VMEM((T, D), bf16),
            dma((U, Y - 1)), dma((U, Y - 1)),
            dma((U, Y - 1, G - 1)), dma((U, Y - 1, G - 1)),
            dma((6,)), dma((6,)),
            dma((U, Y - 1, G)), dma((U, Y - 1, G)),
            dma((6,)),
            dma((2, 2, K, n)), dma((2, K, n)),
            dma((2, K, J, n)), dma((2, 2, K, J, n)),
        ],
        compiler_params=pltpu.CompilerParams(
            collective_id=0, has_side_effects=True, vmem_limit_bytes=VMEM_LIMIT
        ),
    )(
        stream, gain_a.reshape(1, D), gain_b.reshape(1, D),
        gate_a, up_a, down_a, gate_b, up_b, down_b,
    )


def solution(mesh):
    shape = mesh.shape
    in_specs = (
        P(("grp", "fs", "tp"), None),
        P(),
        P("fs", "tp"),
        P("fs", "tp"),
        P("tp", "fs"),
        P(),
        P("fs", "tp"),
        P("fs", "tp"),
        P("tp", "fs"),
    )
    out_specs = P(("grp", "fs", "tp"), None)
    body = functools.partial(local, (shape["grp"], shape["fs"], shape["tp"]))
    return jax.shard_map(body, mesh=mesh, in_specs=in_specs, out_specs=out_specs, check_vma=False)
```

time: 206 us -> 148 us (0.72)
  Pallas kernels: 202 us -> 144 us
    pallas_call x1, Pallas kernels: 202 us -> 144 us  [local(): pl.pallas_call(functools.partial(kernel, (G, m, n, T, D, F, J, K)), out_s...]
where the time goes in v1:
time: 148 us
  Pallas kernels  144 us (97%)
  local copies, waits for them, and re-layouts  3.79 us (3%)
    pallas_call x1, Pallas kernels, local(): pl.pallas_call(functools.partial(kernel, (G, m, n, T, D, F, J, K)), out_s...  144 us

profile of v1, /device:TPU:0, one launch (start us, length us, event | category | flops | bytes accessed | tf_op | source)
XLA Modules:
  0.0 147.9 jit_solution(15303110611105912467)
XLA Ops:
  0.0 0.0 copy-start
  0.0 1.3 reshape.6.gain_a
  1.3 0.0 copy-done
  1.3 0.6 reshape.7.gain_b
  1.9 144.1 %shard_map.91 = bf16[128,2048]{1,0:T(8,128)(2,1)} custom-call(bf16[128,2048]{1,0:T(8,128)(2,1)} %stream.1, bf16[1,2048]{1,0:T(2,128)(2,1)} %reshape.6.gain_a, bf16[1,2048]{1,0:T(2,128)(2,1)} %reshape.7.gain_b, bf16[512,1024]{1,0:T(8,128)(2,1)} %gate_a.1, bf16[512,1024]{1,0:T(8,128)(2,1)} %up_a.1, bf16[1024,512]{1,0:T(8,128)(2,1)} %down_a.1, ...), custom_call_target="tpu_custom_call" | custom-call | tf_op jit(solution)/shard_map/pallas_call | solution.py:402
  146.0 1.9 %copy.11 = bf16[128,2048]{1,0:T(8,128)(2,1)} copy(bf16[128,2048]{1,0:T(8,128)(2,1)} %shard_map.91) | data formatting | bytes 1048576
Async XLA Ops:
  0.0 1.3 copy-start

commit v2 on v1

v2 whole, which is shorter than its diff:
```python
import functools

import jax
import jax.numpy as jnp
from jax import lax
from jax.experimental import pallas as pl
from jax.experimental.pallas import tpu as pltpu
from jax.sharding import PartitionSpec as P

MESH = pl.DeviceIdType.MESH
CORES = 2
PIECES = (8, 8, 8, 4, 4, 4)
UNITS = [(a, p) for a in range(6) for p in range(PIECES[a])]
BATCHES = 4
TUNE = (0.0, (3.35, 4.32), (3.02, 5.12), (7.18, 13.38), (2.82, 6.01), 4.7, 2.0, 2.9)
VMEM_LIMIT = 60 * 1024 * 1024


def kernel(
    sizes,
    stream_hbm, gain_a, gain_b, gate_a, up_a, down_a, gate_b, up_b, down_b,
    out_hbm,
    gu, dn, xg, hid, part, rbuf, acc, mid, stream, out, scale_a, scale_b,
    i_s, o_s, y_s, y_r, x_s, x_r, c_s, c_r, f_s, f_r, l_s, ag_s, ag_r, rs_s, rs_r,
):
    G, m, n, T, D, F, J, K = sizes
    Y = m // CORES
    C = D // J
    R = T // K
    U = len(UNITS)
    gains = (scale_a, scale_b)
    weights = (gate_a, up_a, down_a, gate_b, up_b, down_b)
    g = lax.axis_index("grp")
    fs = lax.axis_index("fs")
    me = lax.axis_index("tp")
    y = fs // CORES
    c = lax.rem(fs, CORES)
    mate = y * CORES + (CORES - 1 - c)
    right = lax.rem(me + 1, n)
    left = lax.rem(me + n - 1, n)

    def row_of(k):
        return lax.rem(y + k + Y, Y) * CORES + c

    def grp_of(i):
        return lax.rem(g + i + G, G)

    def load(k):
        rows = pl.ds(k * R, R)
        return pltpu.make_async_copy(stream_hbm.at[rows, :], stream.at[rows, :], i_s.at[k])

    def save(k):
        rows = pl.ds(k * R, R)
        return pltpu.make_async_copy(out.at[rows, :], out_hbm.at[rows, :], o_s.at[k])

    def gain_load(b):
        return pltpu.make_async_copy((gain_a, gain_b)[b], gains[b], i_s.at[K + b])

    barrier = pltpu.get_barrier_semaphore()
    for k in range(1, Y):
        pl.semaphore_signal(barrier, inc=1, device_id={"fs": row_of(k)}, device_id_type=MESH)
    for i in range(1, G):
        pl.semaphore_signal(barrier, inc=1, device_id={"grp": grp_of(i)}, device_id_type=MESH)
    pl.semaphore_signal(barrier, inc=1, device_id={"fs": mate}, device_id_type=MESH)

    @pl.when(me < n - 1)
    def _():
        pl.semaphore_signal(barrier, inc=1, device_id={"tp": right}, device_id_type=MESH)

    @pl.when(me > 0)
    def _():
        pl.semaphore_signal(barrier, inc=1, device_id={"tp": left}, device_id_type=MESH)

    for k in range(K):
        load(k).start()
    for b in range(2):
        gain_load(b).start()

    @pl.when(jnp.logical_and(me > 0, me < n - 1))
    def _():
        pl.semaphore_wait(barrier, Y - 1 + G - 1 + 1 + 2)

    @pl.when(jnp.logical_not(jnp.logical_and(me > 0, me < n - 1)))
    def _():
        pl.semaphore_wait(barrier, Y - 1 + G - 1 + 1 + 1)

    def rows_of(a):
        return weights[a].shape[0]

    def piece_rows(u, h):
        a, p = UNITS[u]
        rows = rows_of(a) // G
        sub = rows // PIECES[a]
        return pl.multiple_of(h * rows + p * sub, sub), sub

    def own(u, h):
        off, sub = piece_rows(u, h)
        return weights[UNITS[u][0]].at[pl.ds(off, sub), :]

    def place(a, j, off, count):
        b, t = a // 3, a % 3
        if t < 2:
            return gu.at[b, t, pl.ds(pl.multiple_of(j * rows_of(a) + off, count), count), :]
        cols = D // m
        return dn.at[b, pl.ds(off, count), pl.ds(pl.multiple_of(j * cols, cols), cols)]

    def slot(u, j, h):
        off, sub = piece_rows(u, h)
        return place(UNITS[u][0], j, off, sub)

    def whole(a, j):
        return place(a, j, 0, rows_of(a))

    def remote(src, dst, ss, rs, dev):
        return pltpu.make_async_remote_copy(
            src_ref=src, dst_ref=dst, send_sem=ss, recv_sem=rs, device_id=dev, device_id_type=MESH
        )

    def local_copy(a):
        return pltpu.make_async_copy(weights[a], whole(a, fs), l_s.at[a])

    def y_copy(a, k):
        return remote(own(a, g), slot(a, fs, g), y_s, y_r.at[a, k - 1], {"fs": row_of(k)})

    def y_arrived(a, k):
        remote(own(a, g), slot(a, row_of(-k), g), y_s, y_r.at[a, k - 1], {"fs": row_of(k)}).wait_recv()

    def c_copy(a):
        return remote(weights[a], whole(a, fs), c_s, c_r.at[a], {"fs": mate})

    def c_arrived(a):
        remote(weights[a], whole(a, mate), c_s, c_r.at[a], {"fs": mate}).wait_recv()

    def x_copy(a, k, i):
        where = slot(a, row_of(-k), g)
        return remote(where, where, x_s, x_r.at[a, k - 1, i - 1], {"grp": grp_of(i)})

    def x_arrived(a, k, i):
        where = slot(a, row_of(-k), grp_of(-i))
        remote(where, where, x_s, x_r.at[a, k - 1, i - 1], {"grp": grp_of(i)}).wait_recv()

    def f_copy(a, k, i):
        where = slot(a, row_of(-k), grp_of(-i))
        return remote(where, where, f_s, f_r.at[UNITS[a][0]], {"fs": mate})

    def y_event(a):
        for k in range(1, Y):
            y_arrived(a, k)
            for i in range(1, G):
                x_copy(a, k, i).start()
            f_copy(a, k, 0).start()

    def x_event(a):
        for k in range(1, Y):
            for i in range(1, G):
                x_arrived(a, k, i)
                f_copy(a, k, i).start()

    def nearby(a):
        local_copy(a).wait()
        c_arrived(a)

    far = (Y - 1) * (D // m)

    def complete(a):
        where = gu.at[0, 0, pl.ds(0, far), :]
        remote(where, where, f_s, f_r.at[a], {"fs": mate}).wait_recv()

    def sent():
        for rows, sem in (
            (D // m, c_s), (far // G, y_s), (far // G * (G - 1), x_s), (far, f_s),
        ):
            where = gu.at[:, :, pl.ds(0, 6 * rows // 4), :]
            remote(where, where, sem, f_r.at[0], {"fs": mate}).wait_send()

    def rows_at(blk):
        return pl.ds(pl.multiple_of(blk * R, R), R)

    def cols_at(j):
        return pl.ds(pl.multiple_of(lax.rem(y + j, J) * C, C), C)

    def ag(b, way, k, blk):
        where = xg.at[b, k, rows_at(blk), :]
        return remote(where, where, ag_s.at[b, way], ag_r.at[k, blk], {"tp": right if way == 0 else left})

    def ag_step(b, k, s):
        for way in range(2):
            blk = me - s if way == 0 else me + s

            @pl.when(blk >= 0 if way == 0 else blk < n)
            def _():
                ag(b, way, k, blk).wait_recv()

                @pl.when(me < n - 1 if way == 0 else me > 0)
                def _():
                    ag(b, way, k, blk).start()

    def normalize(b, k, source):
        rows = pl.ds(k * R, R)
        v = source[rows, :].astype(jnp.float32)
        scale = lax.rsqrt(jnp.mean(v * v, axis=-1, keepdims=True) + 1e-06)
        xg[b, k, rows_at(me), :] = (v * scale * gains[b][...].astype(jnp.float32).reshape(1, D)).astype(jnp.bfloat16)

        @pl.when(me < n - 1)
        def _():
            ag(b, 0, k, me).start()

        @pl.when(me > 0)
        def _():
            ag(b, 1, k, me).start()

    def hidden_of(b, k):
        tile = min(512, F)

        @pl.loop(0, F // tile)
        def _(q):
            cols = pl.ds(pl.multiple_of(q * tile, tile), tile)
            x = xg[b, k]
            gate = jnp.dot(x, gu[b, 0, :, cols], preferred_element_type=jnp.float32)
            up = jnp.dot(x, gu[b, 1, :, cols], preferred_element_type=jnp.float32)
            hid[k, :, cols] = (gate / (1.0 + jnp.exp(-gate)) * up).astype(jnp.bfloat16)

    def rs(b, way, k, j, d, last=False):
        arrived = rs_r.at[k, j, n if last and way == 1 else d]
        return remote(
            part.at[b, k, j, rows_at(d), :], rbuf.at[b, way, k, j, rows_at(d), :],
            rs_s.at[b], arrived, {"tp": right if way == 0 else left},
        )

    def partial_of(b, k, j):
        tile = min(512, C)

        @pl.loop(0, C // tile)
        def _(q):
            cols = pl.ds(pl.multiple_of(lax.rem(y + j, J) * C + q * tile, tile), tile)
            dst = pl.ds(pl.multiple_of(q * tile, tile), tile)
            part[b, k, j, :, dst] = jnp.dot(
                hid[k], dn[b, :, cols], preferred_element_type=jnp.float32
            ).astype(jnp.bfloat16)

    def hop(b, k, j, q, e):
        for way in range(2):
            @pl.when(me == (q if way == 0 else n - 1 - q))
            def _():
                d = q + e if way == 0 else n - 1 - q - e
                if q > 0:
                    rs(b, way, k, j, d).wait_recv()
                    part[b, k, j, rows_at(d), :] = (
                        part[b, k, j, rows_at(d), :].astype(jnp.float32)
                        + rbuf[b, way, k, j, rows_at(d), :].astype(jnp.float32)
                    ).astype(jnp.bfloat16)
                rs(b, way, k, j, d, e == 1).start()

    def finish(b, k, j, source, target):
        rows = pl.ds(k * R, R)
        acc[...] = part[b, k, j, rows_at(me), :].astype(jnp.float32)

        @pl.when(me > 0)
        def _():
            rs(b, 0, k, j, me, True).wait_recv()
            acc[...] += rbuf[b, 0, k, j, rows_at(me), :].astype(jnp.float32)

        @pl.when(me < n - 1)
        def _():
            rs(b, 1, k, j, me, True).wait_recv()
            acc[...] += rbuf[b, 1, k, j, rows_at(me), :].astype(jnp.float32)

        target[rows, cols_at(j)] = (
            source[rows, cols_at(j)].astype(jnp.float32) + 0.5 * acc[...]
        ).astype(jnp.bfloat16)

    def gathered(b):
        for way in range(2):
            for i in range(1, n):
                @pl.when(me == (i - 1 if way == 0 else n - i))
                def _():
                    where = xg.at[b, :, pl.ds(0, i * R), :]
                    remote(where, where, ag_s.at[b, way], ag_s.at[b, way], {"fs": mate}).wait_send()

    def ship_done(b):
        where = part.at[b, :, :, pl.ds(0, (n - 1) * R), :]
        remote(where, where, rs_s.at[b], rs_s.at[b], {"fs": mate}).wait_send()

    for u in range(PIECES[0]):
        for k in range(1, Y):
            y_copy(u, k).start()
    for b in range(2):
        gain_load(b).wait()
    for k in range(K):
        load(k).wait()
        normalize(0, k, stream)
    for u in range(PIECES[0], U):
        for k in range(1, Y):
            y_copy(u, k).start()

    for kind, args in plan(n, J, K):
        with jax.named_scope(kind + "_" + "_".join(map(str, args))):
            if kind == "y":
                y_event(*args)
            elif kind == "x":
                x_event(*args)
            elif kind == "c":
                complete(*args)
            elif kind == "o":
                nearby(*args)
            elif kind == "a":
                ag_step(*args)
            elif kind == "h":
                hidden_of(*args)
            elif kind == "p":
                partial_of(*args)
            elif kind == "r":
                hop(*args)
            elif kind == "f":
                finish(*args, *((stream, mid) if args[0] == 0 else (mid, out)))
            elif kind == "n":
                normalize(*args, mid)
            elif kind == "s":
                save(*args).start()
            elif kind == "d":
                sent()
            elif kind == "g":
                gathered(*args)
            elif kind == "t":
                ship_done(*args)
            elif kind == "l":
                local_copy(*args).start()
                c_copy(*args).start()

    ship_done(1)
    for k in range(K):
        save(k).wait()


def plan(n, J, K, tune=TUNE):
    items = []

    def at(time, kind, *args):
        items.append((time, len(items), kind, args))

    b0, slots, lag, ends, hops, late, own, early = tune
    whole = J * K
    ready = []
    came = 0
    for u, (a, p) in enumerate(UNITS):
        tau = whole / PIECES[a]
        came += tau
        delay = early if a < 2 else late
        at(came + 0.8, "y", u)
        at(came + tau + delay, "x", u)
        if p == PIECES[a] - 1:
            ready.append(came + tau + delay + 0.1)
    for s in range(1, n):
        for k in range(K):
            at(whole * (s - 1) + J * (k + 1) + 0.9, "a", 0, k, s)
    for a in range(6):
        at(ready[a + 1 if a % 3 == 0 else a], "c", a)
        at(a * own, "l", a)
        at(ready[1] if a < 3 else ready[4], "o", a)
    arrived = [whole * (n - 2) + J * (k + 1) + 1.0 for k in range(K)]
    for b in range(2):
        first = min(3, K) if b == 0 else min(2, K)
        order = [(k, 0) for k in range(first)] + [(k, j) for k in range(first) for j in range(1, J)]
        order += [(k, j) for k in range(first, K) for j in range(J)]
        begun = set()
        done = [0] * K
        now = ready[1] + b0 if b == 0 else max(now, ready[4])
        for place, (k, j) in enumerate(order):
            now = max(now, arrived[k], ready[3 * b + 2] if j > 0 else 0)
            if k not in begun:
                begun.add(k)
                at(now + 0.01, "h", b, k)
            at(now + 0.02, "p", b, k, j)
            spread = b == 1 and k == K - 1
            for q in range(n - 1):
                for e in range(1, n - q):
                    wide = (n - 1 - q - e) / (n - 1)
                    if spread:
                        wide = wide * J + 0.03
                    at(now + 0.03 + lag[b] * q + wide * slots[b], "r", b, k, j, q, e)
            end = now + ends[b] + (0.01 * j if not spread else J * 0.5)
            at(end, "f", b, k, j)
            done[k] = max(done[k], end)
            now += slots[b]
        for k in range(K):
            if b == 0:
                at(done[k] + 0.03, "n", 1, k)
                for s in range(1, n):
                    at(done[k] + 0.04 + hops[k // ((K + 1) // 2)] * s, "a", 1, k, s)
                arrived[k] = done[k] + 0.05 + hops[k // ((K + 1) // 2)] * (n - 1)
            else:
                at(done[k] + 0.03, "s", k)
    at(now - slots[1], "d")
    for b in range(2):
        at(now - slots[1] * (2 - b), "g", b)
    at(now - slots[1], "t", 0)
    items.sort(key=lambda item: item[:2])
    return [item[2:] for item in items]


def local(sizes_of_mesh, stream, gain_a, gate_a, up_a, down_a, gain_b, gate_b, up_b, down_b):
    G, m, n = sizes_of_mesh
    T, D = stream.shape
    F = gate_a.shape[1]
    Y = m // CORES
    J = Y if Y <= 2 else 1
    K = BATCHES
    U = len(UNITS)
    bf16 = jnp.bfloat16
    anywhere = pl.BlockSpec(memory_space=pl.ANY)
    dma = pltpu.SemaphoreType.DMA
    return pl.pallas_call(
        functools.partial(kernel, (G, m, n, T, D, F, J, K)),
        out_shape=jax.ShapeDtypeStruct((T, D), bf16),
        in_specs=[anywhere] * 9,
        out_specs=anywhere,
        scratch_shapes=[
            pltpu.VMEM((2, 2, D, F), bf16),
            pltpu.VMEM((2, F, D), bf16),
            pltpu.VMEM((2, K, n * T // K, D), bf16),
            pltpu.VMEM((K, n * T // K, F), bf16),
            pltpu.VMEM((2, K, J, n * T // K, D // J), bf16),
            pltpu.VMEM((2, 2, K, J, n * T // K, D // J), bf16),
            pltpu.VMEM((T // K, D // J), jnp.float32),
            pltpu.VMEM((T, D), bf16),
            pltpu.VMEM((T, D), bf16),
            pltpu.VMEM((T, D), bf16),
            pltpu.VMEM((D,), bf16),
            pltpu.VMEM((D,), bf16),
            dma((K + 2,)), dma((K,)),
            dma(()), dma((U, Y - 1)),
            dma(()), dma((U, Y - 1, G - 1)),
            dma(()), dma((6,)),
            dma(()), dma((6,)),
            dma((6,)),
            dma((2, 2)), dma((K, n)),
            dma((2,)), dma((K, J, n + 1)),
        ],
        compiler_params=pltpu.CompilerParams(
            collective_id=0, has_side_effects=True, vmem_limit_bytes=VMEM_LIMIT
        ),
    )(
        stream, gain_a, gain_b,
        gate_a, up_a, down_a, gate_b, up_b, down_b,
    )


def solution(mesh):
    shape = mesh.shape
    in_specs = (
        P(("grp", "fs", "tp"), None),
        P(),
        P("fs", "tp"),
        P("fs", "tp"),
        P("tp", "fs"),
        P(),
        P("fs", "tp"),
        P("fs", "tp"),
        P("tp", "fs"),
    )
    out_specs = P(("grp", "fs", "tp"), None)
    body = functools.partial(local, (shape["grp"], shape["fs"], shape["tp"]))
    return jax.shard_map(body, mesh=mesh, in_specs=in_specs, out_specs=out_specs, check_vma=False)
```

time: 148 us -> 130 us (0.88)
  Pallas kernels: 144 us -> 128 us
  local copies, waits for them, and re-layouts: 3.79 us -> 1.88 us
    pallas_call x1, Pallas kernels: 144 us -> 128 us  [local(): pl.pallas_call(functools.partial(kernel, (G, m, n, T, D, F, J, K)), out_s...]
    reshape x2 -> x0, local copies, waits for them, and re-layouts: 1.9 us -> none  [the longest x1 1.3 us: local(): gain_a.reshape(1, D)]
where the time goes in v2:
time: 130 us
  Pallas kernels  128 us (98%)
  local copies, waits for them, and re-layouts  1.88 us (1%)
    pallas_call x1, Pallas kernels, local(): pl.pallas_call(functools.partial(kernel, (G, m, n, T, D, F, J, K)), out_s...  128 us

profile of v2, /device:TPU:0, one launch (start us, length us, event | category | flops | bytes accessed | tf_op | source)
XLA Modules:
  0.0 130.1 jit_solution(2656839726566499398)
XLA Ops:
  0.0 128.2 %shard_map.91 = bf16[128,2048]{1,0:T(8,128)(2,1)} custom-call(bf16[128,2048]{1,0:T(8,128)(2,1)} %stream_hbm.1, bf16[2048]{0:T(1024)(128)(2,1)} %gain_a.1, bf16[2048]{0:T(1024)(128)(2,1)} %gain_b.1, bf16[512,1024]{1,0:T(8,128)(2,1)} %gate_a.1, bf16[512,1024]{1,0:T(8,128)(2,1)} %up_a.1, bf16[1024,512]{1,0:T(8,128)(2,1)} %down_a.1, bf16[512,1024]{1,0:T(8,128)(2,1)} %gate_b.1, ...), custom_call_target="tpu_custom_call" | custom-call | tf_op jit(solution)/shard_map/pallas_call | solution.py:412
  128.2 1.9 %copy.11 = bf16[128,2048]{1,0:T(8,128)(2,1)} copy(bf16[128,2048]{1,0:T(8,128)(2,1)} %shard_map.91) | data formatting | bytes 1048576

commit v3 on v2

--- a/solution.py
+++ b/solution.py
@@ -12,6 +12,22 @@
 PIECES = (8, 8, 8, 4, 4, 4)
 UNITS = [(a, p) for a in range(6) for p in range(PIECES[a])]
 BATCHES = 4
+ORDER = (
+    0, 2, 4, 72, 6, 8, 73, 74, 10, 12, 85, 14, 16, 18, 20, 22, 1, 76, 24, 26,
+    78, 15, 7, 88, 75, 91, 5, 3, 89, 17, 77, 11, 28, 30, 34, 29, 82, 9, 36, 25,
+    31, 23, 32, 27, 21, 19, 13, 84, 92, 87, 80, 86, 102, 38, 103, 105, 106, 81, 40, 111,
+    112, 44, 115, 42, 94, 120, 46, 114, 121, 104, 124, 79, 39, 123, 113, 48, 83, 108, 117, 116,
+    45, 97, 43, 126, 33, 47, 107, 35, 37, 41, 50, 90, 129, 132, 52, 131, 130, 137, 118, 140,
+    49, 109, 134, 145, 139, 127, 133, 54, 125, 119, 153, 110, 122, 135, 148, 162, 56, 142, 136, 170,
+    128, 141, 51, 58, 53, 138, 154, 143, 150, 171, 157, 165, 147, 60, 100, 144, 62, 174, 55, 93,
+    98, 146, 151, 149, 59, 156, 164, 155, 66, 172, 167, 159, 95, 68, 175, 152, 101, 57, 178, 168,
+    63, 61, 173, 96, 158, 64, 186, 70, 160, 187, 176, 163, 189, 166, 190, 65, 261, 188, 161, 67,
+    179, 169, 182, 71, 69, 99, 204, 206, 177, 195, 207, 191, 196, 258, 205, 212, 199, 180, 197, 215,
+    183, 192, 214, 198, 181, 220, 221, 229, 209, 208, 184, 232, 217, 223, 185, 201, 193, 210, 224, 237,
+    194, 200, 231, 238, 241, 246, 234, 202, 249, 213, 211, 226, 218, 260, 248, 216, 240, 203, 243, 251,
+    235, 233, 230, 244, 219, 225, 239, 222, 227, 247, 242, 250, 252, 236, 245, 228, 254, 256, 255, 253,
+    259, 257,
+)
 TUNE = (0.0, (3.35, 4.32), (3.02, 5.12), (7.18, 13.38), (2.82, 6.01), 4.7, 2.0, 2.9)
 VMEM_LIMIT = 60 * 1024 * 1024
 
@@ -394,6 +410,8 @@
     for b in range(2):
         at(now - slots[1] * (2 - b), "g", b)
     at(now - slots[1], "t", 0)
+    if (n, J, K) == (4, 2, 4) and ORDER:
+        return [items[i][2:] for i in ORDER]
     items.sort(key=lambda item: item[:2])
     return [item[2:] for item in items]
 

time: 130 us -> 124 us (0.954)
  Pallas kernels: 128 us -> 122 us
    pallas_call x1, Pallas kernels: 128 us -> 122 us  [local(): pl.pallas_call(functools.partial(kernel, (G, m, n, T, D, F, J, K)), out_s...]
where the time goes in v3:
time: 124 us
  Pallas kernels  122 us (98%)
  local copies, waits for them, and re-layouts  1.88 us (2%)
    pallas_call x1, Pallas kernels, local(): pl.pallas_call(functools.partial(kernel, (G, m, n, T, D, F, J, K)), out_s...  122 us

profile of v3, /device:TPU:0, one launch (start us, length us, event | category | flops | bytes accessed | tf_op | source)
XLA Modules:
  0.0 123.8 jit_solution(5669756395301322523)
XLA Ops:
  0.0 121.9 %shard_map.91 = bf16[128,2048]{1,0:T(8,128)(2,1)} custom-call(bf16[128,2048]{1,0:T(8,128)(2,1)} %stream_hbm.1, bf16[2048]{0:T(1024)(128)(2,1)} %gain_a.1, bf16[2048]{0:T(1024)(128)(2,1)} %gain_b.1, bf16[512,1024]{1,0:T(8,128)(2,1)} %gate_a.1, bf16[512,1024]{1,0:T(8,128)(2,1)} %up_a.1, bf16[1024,512]{1,0:T(8,128)(2,1)} %down_a.1, bf16[512,1024]{1,0:T(8,128)(2,1)} %gate_b.1, ...), custom_call_target="tpu_custom_call" | custom-call | tf_op jit(solution)/shard_map/pallas_call | solution.py:430
  121.9 1.9 %copy.11 = bf16[128,2048]{1,0:T(8,128)(2,1)} copy(bf16[128,2048]{1,0:T(8,128)(2,1)} %shard_map.91) | data formatting | bytes 1048576

commit v4 on v2

--- a/solution.py
+++ b/solution.py
@@ -11,7 +11,27 @@
 CORES = 2
 PIECES = (8, 8, 8, 4, 4, 4)
 UNITS = [(a, p) for a in range(6) for p in range(PIECES[a])]
+DIRECT = (sum(PIECES[:2]) - 1,)
+HELD = sum(PIECES[:2])
+RESUME = HELD - 2
 BATCHES = 4
+ORDER_FOR = (4, 2, 4)
+ORDER = (
+    85, 0, 2, 88, 4, 72, 1, 6, 91, 3, 8, 73, 5, 10, 94, 7, 12, 74, 9, 14,
+    97, 11, 16, 75, 13, 18, 100, 15, 20, 76, 17, 22, 19, 24, 77, 21, 26, 23, 28, 78,
+    25, 30, 27, 79, 31, 86, 89, 92, 32, 29, 80, 84, 87, 102, 34, 95, 103, 106, 81, 36,
+    111, 101, 112, 105, 104, 82, 38, 40, 120, 121, 42, 108, 115, 39, 44, 123, 124, 83, 46, 37,
+    41, 107, 153, 113, 48, 117, 35, 33, 122, 109, 114, 154, 125, 126, 47, 43, 45, 90, 50, 129,
+    132, 131, 110, 118, 137, 145, 162, 127, 98, 140, 134, 52, 133, 130, 54, 142, 116, 148, 146, 128,
+    135, 139, 56, 136, 150, 170, 143, 119, 55, 141, 147, 138, 259, 53, 58, 60, 157, 151, 171, 149,
+    165, 62, 51, 57, 144, 174, 172, 49, 159, 163, 152, 167, 64, 66, 178, 164, 175, 61, 63, 59,
+    93, 68, 173, 96, 186, 156, 168, 187, 188, 190, 160, 70, 166, 158, 176, 155, 189, 69, 65, 179,
+    169, 161, 182, 67, 71, 99, 204, 192, 177, 206, 207, 195, 212, 196, 191, 215, 198, 199, 214, 180,
+    205, 213, 181, 197, 220, 183, 209, 261, 221, 201, 184, 224, 200, 193, 216, 223, 229, 185, 208, 232,
+    202, 237, 194, 246, 210, 217, 249, 238, 241, 248, 226, 203, 240, 225, 231, 234, 211, 218, 251, 247,
+    219, 243, 235, 239, 250, 252, 258, 230, 227, 242, 260, 222, 254, 244, 233, 253, 245, 236, 257, 255,
+    228, 256,
+)
 TUNE = (0.0, (3.35, 4.32), (3.02, 5.12), (7.18, 13.38), (2.82, 6.01), 4.7, 2.0, 2.9)
 VMEM_LIMIT = 60 * 1024 * 1024
 
@@ -19,9 +39,9 @@
 def kernel(
     sizes,
     stream_hbm, gain_a, gain_b, gate_a, up_a, down_a, gate_b, up_b, down_b,
-    out_hbm,
-    gu, dn, xg, hid, part, rbuf, acc, mid, stream, out, scale_a, scale_b,
-    i_s, o_s, y_s, y_r, x_s, x_r, c_s, c_r, f_s, f_r, l_s, ag_s, ag_r, rs_s, rs_r,
+    out,
+    gu, dn, xg, hid, part, rbuf, acc, mid, stream, scale_a, scale_b,
+    i_s, y_s, y_r, x_s, x_r, c_s, c_r, f_s, f_r, l_s, ag_s, ag_r, rs_s, rs_r,
 ):
     G, m, n, T, D, F, J, K = sizes
     Y = m // CORES
@@ -49,10 +69,6 @@
         rows = pl.ds(k * R, R)
         return pltpu.make_async_copy(stream_hbm.at[rows, :], stream.at[rows, :], i_s.at[k])
 
-    def save(k):
-        rows = pl.ds(k * R, R)
-        return pltpu.make_async_copy(out.at[rows, :], out_hbm.at[rows, :], o_s.at[k])
-
     def gain_load(b):
         return pltpu.make_async_copy((gain_a, gain_b)[b], gains[b], i_s.at[K + b])
 
@@ -143,11 +159,22 @@
         where = slot(a, row_of(-k), grp_of(-i))
         return remote(where, where, f_s, f_r.at[UNITS[a][0]], {"fs": mate})
 
+    def y_send(a):
+        for k in range(1, Y):
+            y_copy(a, k).start()
+            for i in range(1, G):
+                if a in DIRECT:
+                    h = grp_of(-i)
+                    remote(
+                        own(a, h), slot(a, fs, h), x_s, x_r.at[a, k - 1, i - 1], {"fs": row_of(k)}
+                    ).start()
+
     def y_event(a):
         for k in range(1, Y):
             y_arrived(a, k)
             for i in range(1, G):
-                x_copy(a, k, i).start()
+                if a not in DIRECT:
+                    x_copy(a, k, i).start()
             f_copy(a, k, 0).start()
 
     def x_event(a):
@@ -282,21 +309,22 @@
         remote(where, where, rs_s.at[b], rs_s.at[b], {"fs": mate}).wait_send()
 
     for u in range(PIECES[0]):
-        for k in range(1, Y):
-            y_copy(u, k).start()
+        y_send(u)
     for b in range(2):
         gain_load(b).wait()
     for k in range(K):
         load(k).wait()
         normalize(0, k, stream)
-    for u in range(PIECES[0], U):
-        for k in range(1, Y):
-            y_copy(u, k).start()
+    for u in range(PIECES[0], HELD):
+        y_send(u)
 
     for kind, args in plan(n, J, K):
         with jax.named_scope(kind + "_" + "_".join(map(str, args))):
             if kind == "y":
                 y_event(*args)
+                if args[0] == RESUME:
+                    for u in range(HELD, U):
+                        y_send(u)
             elif kind == "x":
                 x_event(*args)
             elif kind == "c":
@@ -315,8 +343,6 @@
                 finish(*args, *((stream, mid) if args[0] == 0 else (mid, out)))
             elif kind == "n":
                 normalize(*args, mid)
-            elif kind == "s":
-                save(*args).start()
             elif kind == "d":
                 sent()
             elif kind == "g":
@@ -328,8 +354,6 @@
                 c_copy(*args).start()
 
     ship_done(1)
-    for k in range(K):
-        save(k).wait()
 
 
 def plan(n, J, K, tune=TUNE):
@@ -394,6 +418,8 @@
     for b in range(2):
         at(now - slots[1] * (2 - b), "g", b)
     at(now - slots[1], "t", 0)
+    if (n, J, K) == ORDER_FOR:
+        return [items[i][2:] for i in ORDER]
     items.sort(key=lambda item: item[:2])
     return [item[2:] for item in items]
 
@@ -411,9 +437,9 @@
     dma = pltpu.SemaphoreType.DMA
     return pl.pallas_call(
         functools.partial(kernel, (G, m, n, T, D, F, J, K)),
-        out_shape=jax.ShapeDtypeStruct((T, D), bf16),
+        out_shape=pltpu.VMEM((T, D), bf16),
         in_specs=[anywhere] * 9,
-        out_specs=anywhere,
+        out_specs=pl.BlockSpec(memory_space=pltpu.VMEM),
         scratch_shapes=[
             pltpu.VMEM((2, 2, D, F), bf16),
             pltpu.VMEM((2, F, D), bf16),
@@ -424,10 +450,9 @@
             pltpu.VMEM((T // K, D // J), jnp.float32),
             pltpu.VMEM((T, D), bf16),
             pltpu.VMEM((T, D), bf16),
-            pltpu.VMEM((T, D), bf16),
             pltpu.VMEM((D,), bf16),
             pltpu.VMEM((D,), bf16),
-            dma((K + 2,)), dma((K,)),
+            dma((K + 2,)),
             dma(()), dma((U, Y - 1)),
             dma(()), dma((U, Y - 1, G - 1)),
             dma(()), dma((6,)),

time: 130 us -> 121 us (0.931)
  Pallas kernels: 128 us -> 120 us
    pallas_call x1, Pallas kernels: 128 us -> 120 us  [local(): pl.pallas_call(functools.partial(kernel, (G, m, n, T, D, F, J, K)), out_s...]
where the time goes in v4:
time: 121 us
  Pallas kernels  120 us (99%)
    pallas_call x1, Pallas kernels, local(): pl.pallas_call(functools.partial(kernel, (G, m, n, T, D, F, J, K)), out_s...  120 us

profile of v4, /device:TPU:0, one launch (start us, length us, event | category | flops | bytes accessed | tf_op | source)
XLA Modules:
  0.0 120.6 jit_solution(14996055904301930827)
XLA Ops:
  0.0 119.8 %shard_map.91 = bf16[128,2048]{1,0:T(8,128)(2,1)S(1)} custom-call(bf16[128,2048]{1,0:T(8,128)(2,1)} %stream_hbm.1, bf16[2048]{0:T(1024)(128)(2,1)} %gain_a.1, bf16[2048]{0:T(1024)(128)(2,1)} %gain_b.1, bf16[512,1024]{1,0:T(8,128)(2,1)} %gate_a.1, bf16[512,1024]{1,0:T(8,128)(2,1)} %up_a.1, bf16[1024,512]{1,0:T(8,128)(2,1)} %down_a.1, ...), custom_call_target="tpu_custom_call" | custom-call | tf_op jit(solution)/shard_map/pallas_call | solution.py:438
  119.8 0.8 copy.11

commit v5 on v4

--- a/solution.py
+++ b/solution.py
@@ -23,14 +23,13 @@
     111, 101, 112, 105, 104, 82, 38, 40, 120, 121, 42, 108, 115, 39, 44, 123, 124, 83, 46, 37,
     41, 107, 153, 113, 48, 117, 35, 33, 122, 109, 114, 154, 125, 126, 47, 43, 45, 90, 50, 129,
     132, 131, 110, 118, 137, 145, 162, 127, 98, 140, 134, 52, 133, 130, 54, 142, 116, 148, 146, 128,
-    135, 139, 56, 136, 150, 170, 143, 119, 55, 141, 147, 138, 259, 53, 58, 60, 157, 151, 171, 149,
+    135, 139, 56, 136, 150, 170, 143, 119, 55, 141, 147, 138, 255, 53, 58, 60, 157, 151, 171, 149,
     165, 62, 51, 57, 144, 174, 172, 49, 159, 163, 152, 167, 64, 66, 178, 164, 175, 61, 63, 59,
     93, 68, 173, 96, 186, 156, 168, 187, 188, 190, 160, 70, 166, 158, 176, 155, 189, 69, 65, 179,
     169, 161, 182, 67, 71, 99, 204, 192, 177, 206, 207, 195, 212, 196, 191, 215, 198, 199, 214, 180,
-    205, 213, 181, 197, 220, 183, 209, 261, 221, 201, 184, 224, 200, 193, 216, 223, 229, 185, 208, 232,
+    205, 213, 181, 197, 220, 183, 209, 257, 221, 201, 184, 224, 200, 193, 216, 223, 229, 185, 208, 232,
     202, 237, 194, 246, 210, 217, 249, 238, 241, 248, 226, 203, 240, 225, 231, 234, 211, 218, 251, 247,
-    219, 243, 235, 239, 250, 252, 258, 230, 227, 242, 260, 222, 254, 244, 233, 253, 245, 236, 257, 255,
-    228, 256,
+    219, 243, 235, 239, 250, 252, 254, 230, 227, 242, 256, 222, 244, 233, 253, 245, 236, 228,
 )
 TUNE = (0.0, (3.35, 4.32), (3.02, 5.12), (7.18, 13.38), (2.82, 6.01), 4.7, 2.0, 2.9)
 VMEM_LIMIT = 60 * 1024 * 1024
@@ -402,7 +401,7 @@
                     if spread:
                         wide = wide * J + 0.03
                     at(now + 0.03 + lag[b] * q + wide * slots[b], "r", b, k, j, q, e)
-            end = now + ends[b] + (0.01 * j if not spread else J * 0.5)
+            end = now + max(ends[b], lag[b] * (n - 2) + 0.2, slots[b] * J + 0.2) + (0.01 * j if not spread else J * 0.5)
             at(end, "f", b, k, j)
             done[k] = max(done[k], end)
             now += slots[b]
@@ -412,8 +411,6 @@
                 for s in range(1, n):
                     at(done[k] + 0.04 + hops[k // ((K + 1) // 2)] * s, "a", 1, k, s)
                 arrived[k] = done[k] + 0.05 + hops[k // ((K + 1) // 2)] * (n - 1)
-            else:
-                at(done[k] + 0.03, "s", k)
     at(now - slots[1], "d")
     for b in range(2):
         at(now - slots[1] * (2 - b), "g", b)

time: 121 us -> 121 us (level)
  no operation moved by 1% of the time
where the time goes in v5:
time: 121 us
  Pallas kernels  120 us (99%)
    pallas_call x1, Pallas kernels, local(): pl.pallas_call(functools.partial(kernel, (G, m, n, T, D, F, J, K)), out_s...  120 us

profile of v5, /device:TPU:0, one launch (start us, length us, event | category | flops | bytes accessed | tf_op | source)
XLA Modules:
  0.0 120.6 jit_solution(14996055904301930827)
XLA Ops:
  0.0 119.8 %shard_map.91 = bf16[128,2048]{1,0:T(8,128)(2,1)S(1)} custom-call(bf16[128,2048]{1,0:T(8,128)(2,1)} %stream_hbm.1, bf16[2048]{0:T(1024)(128)(2,1)} %gain_a.1, bf16[2048]{0:T(1024)(128)(2,1)} %gain_b.1, bf16[512,1024]{1,0:T(8,128)(2,1)} %gate_a.1, bf16[512,1024]{1,0:T(8,128)(2,1)} %up_a.1, bf16[1024,512]{1,0:T(8,128)(2,1)} %down_a.1, ...), custom_call_target="tpu_custom_call" | custom-call | tf_op jit(solution)/shard_map/pallas_call | solution.py:435
  119.8 0.8 copy.11
